TPU v7x, 32 devices: a whole 2x2x4 slice. The times are simulated.
32 devices in a mesh: ep: 16 (over z, y, x), tp: 2 (over core).
Axes of the slice: x: 2, y: 2, z: 4, core: 2. Of those that a mesh axis runs over, the one named last changes fastest.
Arguments:
- tokens: bfloat16 [256, 2048], P('ep'), may hold values from -6 to 6
- mix_gain: float32 [2048], replicated, may hold values from 0.1 to 1.9
- query_weight: bfloat16 [2048, 1024], P('ep', 'tp'), may hold values from -0.125 to 0.125
- forget_weight: bfloat16 [2048, 1024], P('ep', 'tp'), may hold values from -0.125 to 0.125
- input_weight: bfloat16 [2048, 1024], P('ep', 'tp'), may hold values from -0.125 to 0.125
- lower_bound: float32 [1024], P('tp'), may hold values from 0 to 0.9
- head_gain: float32 [1024], P('tp'), may hold values from 0.1 to 1.9
- out_weight: bfloat16 [1024, 2048], P('tp', 'ep'), may hold values from -0.1875 to 0.1875
- state: float32 [256, 8, 128, 128], P('ep', 'tp'), may hold values from -4 to 4
- ffn_gain: float32 [2048], replicated, may hold values from 0.1 to 1.9
- route_ids: int32 [256, 2], P('ep'), may hold values from 0 to 7, all different within a row; in each aligned block of 16 rows (0 to 15, 16 to 31, ...) at most 6 rows name the same one
- route_weights: float32 [256, 2], P('ep'), may hold values from 0.25 to 1
- expert_gate: bfloat16 [16, 2048, 2048], P('ep', None, 'tp'), may hold values from -0.125 to 0.125
- expert_up: bfloat16 [16, 2048, 2048], P('ep', None, 'tp'), may hold values from -0.125 to 0.125
- expert_down: bfloat16 [16, 2048, 2048], P('ep', 'tp'), may hold values from -0.09375 to 0.09375
Outputs:
- mixed_out: bfloat16 [256, 2048], P('ep', 'tp')
- new_state: float32 [256, 8, 128, 128], P('ep', 'tp')
Inputs may be any that keep to these rules, and one draw needn't show every extreme that they name: `route_ids`: each row names 2 different experts; among the rows of one device no expert is named by more than 6 rows, a bound that some block reaches of them.
All inputs are finite; a program needn't handle non-finite values.
Results may differ from a plain program's by a relative error of at most 0.015.
Values may be sent and summed in bfloat16 or wider, within the bound.
A program may use at most 64 MiB of HBM per device.

v0:
```python
import jax
import jax.numpy as jnp
from jax import lax
from jax.sharding import PartitionSpec as P

EXPERTS = 8
TOP = 2
epsilon = 1e-06


def rms_scale(values_in, gain_vec):
    return (
        values_in
        * lax.rsqrt(jnp.mean(values_in * values_in, axis=-1, keepdims=True) + epsilon)
        * gain_vec
    )


def slot_ranks(block_ids, expert_count):
    onehot = (block_ids[..., None] == jnp.arange(expert_count, dtype=jnp.int32)).astype(jnp.int32)
    before = jnp.cumsum(onehot, axis=1) - onehot
    return jnp.sum(before * onehot, axis=-1)


def shards(
    tokens,
    mix_gain,
    query_weight,
    forget_weight,
    input_weight,
    lower_bound,
    head_gain,
    out_weight,
    state,
    ffn_gain,
    route_ids,
    route_weights,
    expert_gate,
    expert_up,
    expert_down,
):
    seq_dev = tokens.shape[0]
    model_width = tokens.shape[1]
    ep_count = lax.axis_size("ep")
    residual = tokens.astype(jnp.float32)
    normed = rms_scale(residual, mix_gain).astype(jnp.bfloat16)
    head_count = state.shape[1]
    head_size = state.shape[2]
    proj_width = query_weight.shape[1]
    pieces = (
        lax.all_gather(query_weight, "ep", axis=0, tiled=True),
        lax.all_gather(forget_weight, "ep", axis=0, tiled=True),
        lax.all_gather(input_weight, "ep", axis=0, tiled=True),
    )
    queries, forget_pre, fresh_values = tuple(
        (jnp.dot(normed, weight_rows, preferred_element_type=jnp.float32) for weight_rows in pieces)
    )
    forget = (lower_bound + (1.0 - lower_bound) * jax.nn.sigmoid(forget_pre)).reshape(
        seq_dev, head_count, head_size
    )
    queries = queries.reshape(seq_dev, head_count, head_size)
    fresh_values = fresh_values.reshape(seq_dev, head_count, head_size)
    new_state = forget[..., None] * state + (1.0 - forget)[..., None] * fresh_values[:, :, None, :]
    readout = jnp.einsum("shk,shkv->shv", queries, new_state, precision=lax.Precision.HIGHEST)
    readout = rms_scale(readout, head_gain.reshape(head_count, head_size))
    heads_out = readout.reshape(seq_dev, proj_width).astype(jnp.bfloat16)
    partial_mix = jnp.dot(
        heads_out,
        lax.all_gather(out_weight, "ep", axis=1, tiled=True),
        preferred_element_type=jnp.float32,
    )
    mixer_sum = lax.psum(partial_mix.astype(jnp.bfloat16), "tp").astype(jnp.float32)
    after_mixer = (residual + mixer_sum).astype(jnp.bfloat16)
    ffn_in = rms_scale(after_mixer.astype(jnp.float32), ffn_gain).astype(jnp.bfloat16)
    capacity = 3 * seq_dev // 8
    expert_span = ep_count // EXPERTS
    half_width = model_width // lax.axis_size("tp")
    own_columns = lax.dynamic_slice_in_dim(
        after_mixer, lax.axis_index("tp") * half_width, half_width, 1
    ).astype(jnp.float32)
    gate_slice = expert_gate[0]
    up_slice = expert_up[0]
    down_slice = expert_down[0]
    slot_iota = jnp.arange(capacity, dtype=jnp.int32)
    own_rank = slot_ranks(route_ids.reshape(1, seq_dev * TOP), EXPERTS).reshape(seq_dev, TOP)
    expert_iota = jnp.arange(EXPERTS, dtype=jnp.int32)
    chosen = (route_ids[:, :, None, None] == expert_iota[None, None, :, None]) & (
        own_rank[:, :, None, None] == slot_iota[None, None, None, :]
    )
    dispatch = jnp.any(chosen, axis=1).astype(jnp.bfloat16)
    combine = jnp.sum(chosen.astype(jnp.float32) * route_weights[:, :, None, None], axis=1)
    outgoing = jnp.einsum(
        "tec,td->ecd", dispatch, ffn_in, preferred_element_type=jnp.float32
    ).astype(jnp.bfloat16)
    outgoing = jnp.broadcast_to(
        outgoing[:, None], (EXPERTS, expert_span, capacity, model_width)
    ).reshape(ep_count, capacity, model_width)
    slot_rows = lax.all_to_all(outgoing, "ep", split_axis=0, concat_axis=0, tiled=True)
    gate_pre = jnp.einsum(
        "...d,df->...f", slot_rows, gate_slice, preferred_element_type=jnp.float32
    )
    up_pre = jnp.einsum("...d,df->...f", slot_rows, up_slice, preferred_element_type=jnp.float32)
    hidden = (jax.nn.silu(gate_pre) * up_pre).astype(jnp.bfloat16)
    partial_out = jnp.einsum(
        "...f,fd->...d", hidden, down_slice, preferred_element_type=jnp.float32
    )
    reduced = lax.psum_scatter(
        partial_out.astype(jnp.bfloat16), "tp", scatter_dimension=2, tiled=True
    ).astype(jnp.float32)
    returned = lax.all_to_all(
        reduced.astype(jnp.bfloat16), "ep", split_axis=0, concat_axis=0, tiled=True
    ).astype(reduced.dtype)
    expert_out = jnp.sum(returned.reshape(EXPERTS, expert_span, capacity, half_width), axis=1)
    expert_mix = jnp.einsum("tec,ecd->td", combine, expert_out, precision=lax.Precision.HIGHEST)
    mixed_out = (own_columns + expert_mix).astype(jnp.bfloat16)
    return (mixed_out, new_state)


def solution(mesh):
    return jax.shard_map(
        shards,
        mesh=mesh,
        in_specs=(
            P("ep", None),
            P(),
            P("ep", "tp"),
            P("ep", "tp"),
            P("ep", "tp"),
            P("tp"),
            P("tp"),
            P("tp", "ep"),
            P("ep", "tp", None, None),
            P(),
            P("ep", None),
            P("ep", None),
            P("ep", None, "tp"),
            P("ep", None, "tp"),
            P("ep", "tp", None),
        ),
        out_specs=(P("ep", "tp"), P("ep", "tp", None, None)),
        check_vma=False,
    )
```

profile of v0, /device:TPU:0, one launch (start us, length us, event | category | flops | bytes accessed | tf_op | source)
XLA Modules:
  0.0 346.5 jit_solution(2052995556414389581)
XLA Ops:
  8.0 0.7 all-gather.9.cloned.1.call-update
  10.0 0.8 copy.47
  11.4 1.0 fusion.37
  13.7 60.2 %all-gather.7.cloned.1.call-done = bf16[2048,512]{1,0:T(8,128)(2,1)} async-done(((bf16[128,512]{1,0:T(8,128)(2,1)}), bf16[2048,512]{1,0:T(8,128)(2,1)}) %all-gather.7.cloned.1.call-update) | async-done | bytes 2097168 | tf_op jit(solution)/shard_map/all_gather | solution.py:52
  73.9 2.1 fusion.21
  76.0 59.9 %all-gather.9.cloned.1.call-done = bf16[2048,512]{1,0:T(8,128)(2,1)} async-done(((bf16[128,512]{1,0:T(8,128)(2,1)}), bf16[2048,512]{1,0:T(8,128)(2,1)}) %all-gather.9.cloned.1.call-update) | async-done | bytes 2097168 | tf_op jit(solution)/shard_map/all_gather | solution.py:53
  135.9 2.1 fusion.50
  138.0 59.9 %all-gather.5.cloned.1.call-done = bf16[2048,512]{1,0:T(8,128)(2,1)} async-done(((bf16[128,512]{1,0:T(8,128)(2,1)}), bf16[2048,512]{1,0:T(8,128)(2,1)}) %all-gather.5.cloned.1.call-update) | async-done | bytes 2097168 | tf_op jit(solution)/shard_map/all_gather | solution.py:51
  197.9 2.0 fusion.53
  199.9 4.4 %multiply_add_fusion = f32[16,4,128,128]{3,2,1,0:T(8,128)S(1)} fusion(f32[16,4,128,128]{3,2,1,0:T(8,128)} %param.23, f32[16,4,128]{2,1,0:T(4,128)S(1)} %mul.124, f32[16,4,128]{2,1,0:T(4,128)S(1)} %broadcast_subtract_fusion, f32[16,4,128]{2,1,0:T(4,128)S(1)} %mul.120), kind=kLoop, calls=%fused_computation.6 | loop fusion | flops 3145728 | bytes 8486912 | tf_op jit(solution)/shard_map/add | solution.py:63
  204.4 2.0 copy-done
  206.3 3.7 %fusion.56 = f32[16,4,1,128]{3,2,1,0:T(1,128)S(1)} fusion(f32[16,4,128,1]{2,3,1,0:T(1,128)S(1)} %bitcast.52, f32[16,4,128,128]{3,2,1,0:T(8,128)S(1)} %multiply_add_fusion), kind=kOutput, calls=%fused_computation.66 | convolution fusion | flops 12582912 | bytes 4259840 | tf_op jit(solution)/shard_map/shk,shkv->shv/dot_general | solution.py:64
  210.2 52.0 %all-gather.11.cloned.1.call-done = bf16[512,2048]{1,0:T(8,128)(2,1)} async-done(((bf16[512,128]{1,0:T(8,128)(2,1)}), bf16[512,2048]{1,0:T(8,128)(2,1)}) %all-gather.11.cloned.1.call-update) | async-done | bytes 2097168 | tf_op jit(solution)/shard_map/all_gather | solution.py:69
  262.2 2.6 convolution_convert_fusion.1
  264.9 16.0 %all-reduce.2.cloned.1.call-done = bf16[16,2048]{1,0:T(8,128)(2,1)} async-done(((bf16[16,2048]{1,0:T(8,128)(2,1)}), bf16[16,2048]{1,0:T(8,128)(2,1)}) %all-reduce.2.cloned.1.call-update) | async-done | bytes 65552 | tf_op jit(solution)/shard_map/psum | solution.py:72
  280.9 1.0 fusion.34
  282.3 22.1 %all_to_all.10 = bf16[16,6,2048]{2,1,0:T(8,128)(2,1)S(1)} all-to-all(bf16[16,6,2048]{2,1,0:T(8,128)(2,1)S(1)} %bitcast.49), channel_id=1, replica_groups=mesh['ep'=16,'tp'=2] {'ep'}, dimensions={0} | all-to-all | bytes 786432 | tf_op jit(solution)/shard_map/all_to_all | solution.py:98
  304.4 3.1 fusion.4
  307.5 5.9 %fusion.6 = bf16[16,6,2048]{2,0,1:T(8,128)(2,1)} fusion(bf16[1,1024,2048]{2,1,0:T(8,128)(2,1)} %param.29, bf16[1,2048,1024]{2,1,0:T(8,128)(2,1)} %param.28, f32[16,6,1024]{2,0,1:T(8,128)S(1)} %fusion.4, bf16[16,6,2048]{2,1,0:T(8,128)(2,1)S(1)} %all_to_all.10), kind=kOutput, calls=%fused_computation.7 | convolution fusion | flops 806092800 | bytes 9568256 | tf_op jit(solution)/shard_map/...f,fd->...d/dot_general | solution.py:104
  313.4 6.3 %reduce-scatter.2.cloned.1.call-done = bf16[16,6,1024]{2,0,1:T(8,128)(2,1)} async-done(((bf16[16,6,2048]{2,0,1:T(8,128)(2,1)}), bf16[16,6,1024]{2,0,1:T(8,128)(2,1)}) %reduce-scatter.2.cloned.1.call-update) | async-done | bytes 196624 | tf_op jit(solution)/shard_map/reduce_scatter | solution.py:107
  319.8 1.7 copy.52
  321.5 6.7 %all-to-all-start.1 = ((bf16[16,6,1024]{2,1,0:T(8,128)(2,1)}), bf16[16,6,1024]{2,1,0:T(8,128)(2,1)S(1)}, u32[]{:S(2)}, u32[]{:S(2)}) async-start(bf16[16,6,1024]{2,1,0:T(8,128)(2,1)} %copy.52), calls=%async_computation.2 | async-start | bytes 524288 | tf_op jit(solution)/shard_map/all_to_all | solution.py:110
  328.3 10.4 %all-to-all-done.1 = bf16[16,6,1024]{2,1,0:T(8,128)(2,1)S(1)} async-done(((bf16[16,6,1024]{2,1,0:T(8,128)(2,1)}), bf16[16,6,1024]{2,1,0:T(8,128)(2,1)S(1)}, u32[]{:S(2)}, u32[]{:S(2)}) %all-to-all-start.1) | async-done | bytes 196640 | tf_op jit(solution)/shard_map/all_to_all | solution.py:110
  338.7 0.9 fusion.16
  (46 shorter events, 4.9 us)
Async XLA Ops:
  7.2 190.7 %copy-start.1 = (bf16[16,2048]{1,0:T(8,128)(2,1)S(1)}, bf16[16,2048]{1,0:T(8,128)(2,1)}, u32[]{:S(2)}) copy-start(bf16[16,2048]{1,0:T(8,128)(2,1)} %param.15) | copy-start | bytes 196612
  7.2 190.7 %copy-start.2 = (f32[2048]{0:T(1024)S(1)}, f32[2048]{0:T(1024)}, u32[]{:S(2)}) copy-start(f32[2048]{0:T(1024)} %param.16) | copy-start | bytes 24580
  7.2 66.7 %all-gather.7.cloned.1.call-start = ((), (), s32[]{:S(2)}) async-start(), calls=%async_computation.4 | async-start | bytes 2228224 | tf_op jit(solution)/shard_map/all_gather | solution.py:52
  7.9 128.0 %all-gather.9.cloned.1.call-start = ((), (), s32[]{:S(2)}) async-start(), calls=%async_computation.5 | async-start | bytes 2228224 | tf_op jit(solution)/shard_map/all_gather | solution.py:53
  8.7 189.2 %all-gather.5.cloned.1.call-start = ((), (), s32[]{:S(2)}) async-start(), calls=%async_computation.3 | async-start | bytes 2228224 | tf_op jit(solution)/shard_map/all_gather | solution.py:51
  9.4 252.8 %all-gather.11.cloned.1.call-start = ((), (), s32[]{:S(2)}) async-start(), calls=%async_computation.6 | async-start | bytes 2228224 | tf_op jit(solution)/shard_map/all_gather | solution.py:69
  10.0 270.9 %all-reduce.2.cloned.1.call-start = ((), (), s32[]{:S(2)}) async-start(), calls=%async_computation.7 | async-start | bytes 131072 | tf_op jit(solution)/shard_map/psum | solution.py:72
  204.3 2.0 copy-start
  204.3 5.8 %copy-start.4 = (f32[512]{0:T(512)S(1)}, f32[512]{0:T(512)}, u32[]{:S(2)}) copy-start(f32[512]{0:T(512)} %param.21) | copy-start | bytes 6148
  204.4 77.5 %copy-start.3 = (f32[2048]{0:T(1024)S(1)}, f32[2048]{0:T(1024)}, u32[]{:S(2)}) copy-start(f32[2048]{0:T(1024)} %param.24) | copy-start | bytes 24580
  264.8 55.0 %reduce-scatter.2.cloned.1.call-start = ((), (), s32[]{:S(2)}) async-start(), calls=%async_computation.8 | async-start | bytes 589824 | tf_op jit(solution)/shard_map/reduce_scatter | solution.py:107
  307.5 20.7 %copy-start.5 = (f32[16,2]{0,1:T(2,128)S(1)}, f32[16,2]{0,1:T(2,128)}, u32[]{:S(2)}) copy-start(f32[16,2]{0,1:T(2,128)} %param.26) | copy-start | bytes 388
  321.5 17.1 %all-to-all-start.1 = ((bf16[16,6,1024]{2,1,0:T(8,128)(2,1)}), bf16[16,6,1024]{2,1,0:T(8,128)(2,1)S(1)}, u32[]{:S(2)}, u32[]{:S(2)}) async-start(bf16[16,6,1024]{2,1,0:T(8,128)(2,1)} %copy.52), calls=%async_computation.2 | async-start | bytes 524288 | tf_op jit(solution)/shard_map/all_to_all | solution.py:110
Sparse Core Ops, SparseCore 0:
  10.8 63.0 all-gather.6
  76.7 59.1 all-gather.8
  138.7 59.1 all-gather.4
  200.4 61.7 all-gather.10
  264.9 15.8 all-reduce.1
  313.6 6.1 reduce-scatter.1
where the time goes:
time: 347 us; the launch traced here: 346 us
  waiting for transfers between devices  267 us (77%)
  matrix products  22.6 us (7%)
  blocking collectives  22.1 us (6%)
  between operations  14.3 us (4%)
  other arithmetic  8.35 us (2%)
  starting transfers between devices  6.96 us (2%)
  local copies, waits for them, and re-layouts  4.97 us (1%)
    all_gather x1, waiting for transfers between devices, shards(): lax.all_gather(forget_weight, 'ep', axis=0, tiled=True)  60.2 us
    all_gather x1, waiting for transfers between devices, shards(): lax.all_gather(query_weight, 'ep', axis=0, tiled=True)  59.9 us
    all_gather x1, waiting for transfers between devices, shards(): lax.all_gather(input_weight, 'ep', axis=0, tiled=True)  59.9 us
    all_gather x1, waiting for transfers between devices, shards(): lax.all_gather(out_weight, 'ep', axis=1, tiled=True)  52 us
    all_to_all x1, blocking collectives, shards(): lax.all_to_all(outgoing, 'ep', split_axis=0, concat_axis=0, tiled=True)  22.1 us
    psum x1, waiting for transfers between devices, shards(): lax.psum(partial_mix.astype(jnp.bfloat16), 'tp').astype(jnp.float32)  16 us
    all_to_all x1, waiting for transfers between devices, shards(): lax.all_to_all(reduced.astype(jnp.bfloat16), 'ep', split_axis=0, concat_a...  10.4 us
  transfers between devices with their start and end apart: 7, of which 7 were waited for; matrix products, arithmetic and copies ran while one was open for 5% of the time, Pallas kernels for 0%

commit v1 on v0

--- a/solution.py
+++ b/solution.py
@@ -66,7 +66,7 @@
     heads_out = readout.reshape(seq_dev, proj_width).astype(jnp.bfloat16)
     partial_mix = jnp.dot(
         heads_out,
-        lax.all_gather(out_weight, "ep", axis=1, tiled=True),
+        jnp.concatenate(jax.lax.all_gather(out_weight, "ep"), 1),
         preferred_element_type=jnp.float32,
     )
     mixer_sum = lax.psum(partial_mix.astype(jnp.bfloat16), "tp").astype(jnp.float32)

time: 347 us -> 356 us (1.026)
  waiting for transfers between devices: 267 us -> 275 us
    all_gather x1, waiting for transfers between devices: 52 us -> 60.2 us  [shards(): jax.lax.all_gather(out_weight, 'ep')]
  transfers between devices with their start and end apart: 7 -> 7, of which waited for: 7 -> 7; matrix products, arithmetic and copies ran while one was open for 5% -> 3% of each run, Pallas kernels for 0% -> 0%
where the time goes in v1:
time: 356 us
  waiting for transfers between devices  275 us (77%)
  blocking collectives  22.1 us (6%)
  matrix products  21.1 us (6%)
  between operations  14.3 us (4%)
  other arithmetic  8.34 us (2%)
  local copies, waits for them, and re-layouts  7.84 us (2%)
  starting transfers between devices  6.95 us (2%)
    all_gather x1, waiting for transfers between devices, shards(): jax.lax.all_gather(out_weight, 'ep')  60.2 us
    all_gather x1, waiting for transfers between devices, shards(): lax.all_gather(input_weight, 'ep', axis=0, tiled=True)  59.9 us
    all_gather x1, waiting for transfers between devices, shards(): lax.all_gather(forget_weight, 'ep', axis=0, tiled=True)  59.8 us
    all_gather x1, waiting for transfers between devices, shards(): lax.all_gather(query_weight, 'ep', axis=0, tiled=True)  59.1 us
    all_to_all x1, blocking collectives, shards(): lax.all_to_all(outgoing, 'ep', split_axis=0, concat_axis=0, tiled=True)  22.1 us
    psum x1, waiting for transfers between devices, shards(): lax.psum(partial_mix.astype(jnp.bfloat16), 'tp').astype(jnp.float32)  16.6 us
    all_to_all x1, waiting for transfers between devices, shards(): lax.all_to_all(reduced.astype(jnp.bfloat16), 'ep', split_axis=0, concat_a...  10.3 us
  transfers between devices with their start and end apart: 7, of which 7 were waited for; matrix products, arithmetic and copies ran while one was open for 3% of the time, Pallas kernels for 0%

profile of v1, /device:TPU:0, one launch (start us, length us, event | category | flops | bytes accessed | tf_op | source)
XLA Modules:
  0.0 355.6 jit_solution(10672729184195997613)
XLA Ops:
  10.0 0.8 copy.55
  11.4 1.0 fusion.37
  13.7 60.2 %all-gather.12.cloned.1.call-done = bf16[8192,128]{1,0:T(8,128)(2,1)} async-done(((bf16[512,128]{1,0:T(8,128)(2,1)}), bf16[8192,128]{1,0:T(8,128)(2,1)}) %all-gather.12.cloned.1.call-update) | async-done | bytes 2097168 | tf_op jit(solution)/shard_map/all_gather | solution.py:69
  73.9 2.9 copy.54
  76.8 59.1 %all-gather.6.cloned.1.call-done = bf16[2048,512]{1,0:T(8,128)(2,1)} async-done(((bf16[128,512]{1,0:T(8,128)(2,1)}), bf16[2048,512]{1,0:T(8,128)(2,1)}) %all-gather.6.cloned.1.call-update) | async-done | bytes 2097168 | tf_op jit(solution)/shard_map/all_gather | solution.py:51
  135.9 2.0 fusion.53
  137.9 59.9 %all-gather.10.cloned.1.call-done = bf16[2048,512]{1,0:T(8,128)(2,1)} async-done(((bf16[128,512]{1,0:T(8,128)(2,1)}), bf16[2048,512]{1,0:T(8,128)(2,1)}) %all-gather.10.cloned.1.call-update) | async-done | bytes 2097168 | tf_op jit(solution)/shard_map/all_gather | solution.py:53
  197.9 2.0 fusion.50
  199.9 59.8 %all-gather.8.cloned.1.call-done = bf16[2048,512]{1,0:T(8,128)(2,1)} async-done(((bf16[128,512]{1,0:T(8,128)(2,1)}), bf16[2048,512]{1,0:T(8,128)(2,1)}) %all-gather.8.cloned.1.call-update) | async-done | bytes 2097168 | tf_op jit(solution)/shard_map/all_gather | solution.py:52
  259.7 2.0 fusion.21
  261.8 4.4 %multiply_add_fusion = f32[16,4,128,128]{3,2,1,0:T(8,128)S(1)} fusion(f32[16,4,128,128]{3,2,1,0:T(8,128)} %param.23, f32[16,4,128]{2,1,0:T(4,128)S(1)} %mul.124, f32[16,4,128]{2,1,0:T(4,128)S(1)} %broadcast_subtract_fusion, f32[16,4,128]{2,1,0:T(4,128)S(1)} %mul.120), kind=kLoop, calls=%fused_computation.6 | loop fusion | flops 3145728 | bytes 8486912 | tf_op jit(solution)/shard_map/add | solution.py:63
  266.2 2.0 copy-done
  268.2 3.7 %fusion.56 = f32[16,4,1,128]{3,2,1,0:T(1,128)S(1)} fusion(f32[16,4,128,1]{2,3,1,0:T(1,128)S(1)} %bitcast.58, f32[16,4,128,128]{3,2,1,0:T(8,128)S(1)} %multiply_add_fusion), kind=kOutput, calls=%fused_computation.66 | convolution fusion | flops 12582912 | bytes 4259840 | tf_op jit(solution)/shard_map/shk,shkv->shv/dot_general | solution.py:64
  272.1 1.3 convolution_convert_fusion.1
  273.4 16.6 %all-reduce.2.cloned.1.call-done = bf16[16,2048]{1,0:T(8,128)(2,1)} async-done(((bf16[16,2048]{1,0:T(8,128)(2,1)}), bf16[16,2048]{1,0:T(8,128)(2,1)}) %all-reduce.2.cloned.1.call-update) | async-done | bytes 65552 | tf_op jit(solution)/shard_map/psum | solution.py:72
  290.0 1.0 fusion.34
  291.5 22.1 %all_to_all.10 = bf16[16,6,2048]{2,1,0:T(8,128)(2,1)S(1)} all-to-all(bf16[16,6,2048]{2,1,0:T(8,128)(2,1)S(1)} %bitcast.55), channel_id=1, replica_groups=mesh['ep'=16,'tp'=2] {'ep'}, dimensions={0} | all-to-all | bytes 786432 | tf_op jit(solution)/shard_map/all_to_all | solution.py:98
  313.6 3.1 fusion.4
  316.7 5.9 %fusion.6 = bf16[16,6,2048]{2,0,1:T(8,128)(2,1)} fusion(bf16[1,1024,2048]{2,1,0:T(8,128)(2,1)} %param.29, bf16[1,2048,1024]{2,1,0:T(8,128)(2,1)} %param.28, f32[16,6,1024]{2,0,1:T(8,128)S(1)} %fusion.4, bf16[16,6,2048]{2,1,0:T(8,128)(2,1)S(1)} %all_to_all.10), kind=kOutput, calls=%fused_computation.7 | convolution fusion | flops 806092800 | bytes 9568256 | tf_op jit(solution)/shard_map/...f,fd->...d/dot_general | solution.py:104
  322.6 6.3 %reduce-scatter.2.cloned.1.call-done = bf16[16,6,1024]{2,0,1:T(8,128)(2,1)} async-done(((bf16[16,6,2048]{2,0,1:T(8,128)(2,1)}), bf16[16,6,1024]{2,0,1:T(8,128)(2,1)}) %reduce-scatter.2.cloned.1.call-update) | async-done | bytes 196624 | tf_op jit(solution)/shard_map/reduce_scatter | solution.py:107
  328.9 1.7 copy.60
  330.7 6.7 %all-to-all-start.1 = ((bf16[16,6,1024]{2,1,0:T(8,128)(2,1)}), bf16[16,6,1024]{2,1,0:T(8,128)(2,1)S(1)}, u32[]{:S(2)}, u32[]{:S(2)}) async-start(bf16[16,6,1024]{2,1,0:T(8,128)(2,1)} %copy.60), calls=%async_computation.2 | async-start | bytes 524288 | tf_op jit(solution)/shard_map/all_to_all | solution.py:110
  337.4 10.3 %all-to-all-done.1 = bf16[16,6,1024]{2,1,0:T(8,128)(2,1)S(1)} async-done(((bf16[16,6,1024]{2,1,0:T(8,128)(2,1)}), bf16[16,6,1024]{2,1,0:T(8,128)(2,1)S(1)}, u32[]{:S(2)}, u32[]{:S(2)}) %all-to-all-start.1) | async-done | bytes 196640 | tf_op jit(solution)/shard_map/all_to_all | solution.py:110
  347.8 0.9 fusion.16
  (49 shorter events, 5.6 us)
Async XLA Ops:
  7.2 128.7 %copy-start.1 = (bf16[16,2048]{1,0:T(8,128)(2,1)S(1)}, bf16[16,2048]{1,0:T(8,128)(2,1)}, u32[]{:S(2)}) copy-start(bf16[16,2048]{1,0:T(8,128)(2,1)} %param.15) | copy-start | bytes 196612
  7.2 128.7 %copy-start.2 = (f32[2048]{0:T(1024)S(1)}, f32[2048]{0:T(1024)}, u32[]{:S(2)}) copy-start(f32[2048]{0:T(1024)} %param.16) | copy-start | bytes 24580
  7.2 66.7 %all-gather.12.cloned.1.call-start = ((), (), s32[]{:S(2)}) async-start(), calls=%async_computation.8 | async-start | bytes 2228224 | tf_op jit(solution)/shard_map/all_gather | solution.py:69
  7.9 128.0 %all-gather.6.cloned.1.call-start = ((), (), s32[]{:S(2)}) async-start(), calls=%async_computation.3 | async-start | bytes 2228224 | tf_op jit(solution)/shard_map/all_gather | solution.py:51
  8.7 189.2 %all-gather.10.cloned.1.call-start = ((), (), s32[]{:S(2)}) async-start(), calls=%async_computation.5 | async-start | bytes 2228224 | tf_op jit(solution)/shard_map/all_gather | solution.py:53
  9.4 250.3 %all-gather.8.cloned.1.call-start = ((), (), s32[]{:S(2)}) async-start(), calls=%async_computation.4 | async-start | bytes 2228224 | tf_op jit(solution)/shard_map/all_gather | solution.py:52
  10.0 280.1 %all-reduce.2.cloned.1.call-start = ((), (), s32[]{:S(2)}) async-start(), calls=%async_computation.6 | async-start | bytes 131072 | tf_op jit(solution)/shard_map/psum | solution.py:72
  73.9 185.8 %copy-start.3 = (f32[512]{0:T(512)S(1)}, f32[512]{0:T(512)}, u32[]{:S(2)}) copy-start(f32[512]{0:T(512)} %param.20) | copy-start | bytes 6148
  266.2 2.0 copy-start
  266.2 5.8 %copy-start.5 = (f32[512]{0:T(512)S(1)}, f32[512]{0:T(512)}, u32[]{:S(2)}) copy-start(f32[512]{0:T(512)} %param.21) | copy-start | bytes 6148
  266.2 24.8 %copy-start.4 = (f32[2048]{0:T(1024)S(1)}, f32[2048]{0:T(1024)}, u32[]{:S(2)}) copy-start(f32[2048]{0:T(1024)} %param.24) | copy-start | bytes 24580
  273.4 55.6 %reduce-scatter.2.cloned.1.call-start = ((), (), s32[]{:S(2)}) async-start(), calls=%async_computation.7 | async-start | bytes 589824 | tf_op jit(solution)/shard_map/reduce_scatter | solution.py:107
  316.7 20.7 %copy-start.6 = (f32[16,2]{0,1:T(2,128)S(1)}, f32[16,2]{0,1:T(2,128)}, u32[]{:S(2)}) copy-start(f32[16,2]{0,1:T(2,128)} %param.26) | copy-start | bytes 388
  330.7 17.1 %all-to-all-start.1 = ((bf16[16,6,1024]{2,1,0:T(8,128)(2,1)}), bf16[16,6,1024]{2,1,0:T(8,128)(2,1)S(1)}, u32[]{:S(2)}, u32[]{:S(2)}) async-start(bf16[16,6,1024]{2,1,0:T(8,128)(2,1)} %copy.60), calls=%async_computation.2 | async-start | bytes 524288 | tf_op jit(solution)/shard_map/all_to_all | solution.py:110
Sparse Core Ops, SparseCore 0:
  10.8 63.0 all-gather.11
  76.7 59.1 all-gather.5
  138.7 59.1 all-gather.9
  200.5 59.1 all-gather.7
  273.5 16.4 all-reduce.1
  322.7 6.1 reduce-scatter.1
